TPU v7x, 32 devices: a whole 2x2x4 slice. The times are simulated.
32 devices in a mesh: ep: 8 (over z, x), tp: 4 (over y, core).
Axes of the slice: x: 2, y: 2, z: 4, core: 2. Of those that a mesh axis runs over, the one named last changes fastest.
Arguments:
- filter_value: bfloat16 [8192, 1024], P(('ep', 'tp')), may hold values from -6 to 6
- filter_gate: bfloat16 [8192, 1024], P(('ep', 'tp')), may hold values from -9 to 9
- filter_taps: float32 [31, 1024], replicated, may hold values from -1 to 1
- filter_bias: float32 [1024], replicated, may hold values from -3 to 3
- norm_gain: float32 [1024], replicated, may hold values from 0.1 to 1.9
- norm_shift: float32 [1024], replicated, may hold values from -3 to 3
- out_weight: bfloat16 [1024, 2048], replicated, may hold values from -0.1875 to 0.1875
- out_bias: float32 [2048], replicated, may hold values from -3 to 3
- expert_input: bfloat16 [2048, 2048], P('ep'), may hold values from -6 to 6
- expert_gain: float32 [2048], replicated, may hold values from 0.1 to 1.9
- route_experts: int32 [2048, 2], P('ep'), may hold values from 0 to 7, all different within a row; in each aligned block of 256 rows (0 to 255, 256 to 511, ...) at most 128 rows name the same one
- route_weights: float32 [2048, 2], P('ep'), may hold values from 0.2 to 1
- gate_weights: bfloat16 [8, 2048, 2048], P('ep', None, 'tp'), may hold values from -0.375 to 0.375
- up_weights: bfloat16 [8, 2048, 2048], P('ep', None, 'tp'), may hold values from -0.375 to 0.375
- down_weights: bfloat16 [8, 2048, 2048], P('ep', 'tp'), may hold values from -0.0234375 to 0.0234375
Outputs:
- mixer_out: bfloat16 [8192, 2048], P(('ep', 'tp'))
- expert_out: bfloat16 [2048, 2048], P('ep', 'tp')
Inputs may be any that keep to these rules, and one draw needn't show every extreme that they name: `route_experts`: each row names 2 different experts. Within the rows of one index of ep (aligned blocks of 256 rows) no expert is named by more than 128 rows, a bound that some block reaches.
All inputs are finite; a program needn't handle non-finite values.
Results may differ from a plain program's by a relative error of at most 0.012.
Values may be sent and summed in bfloat16 or wider, within the bound.
A program may use at most 128 MiB of HBM per device.

v0:
```python
import functools

import jax
import jax.numpy as jnp
from jax import lax
from jax.experimental import pallas as pl
from jax.experimental.pallas import tpu as pltpu
from jax.sharding import PartitionSpec as P

epsilon = 1e-06
clamp_limit = 7.0
swish_alpha = 1.702
LANES = 128
f32 = jnp.float32
bf16 = jnp.bfloat16


def dot(a, b):
    return jnp.dot(a, b, preferred_element_type=f32)


def kernel(
    n_ep,
    n_tp,
    capacity,
    value_hbm,
    gate_hbm,
    taps_ref,
    bias_ref,
    gain_ref,
    shift_ref,
    out_weight_hbm,
    out_bias_ref,
    tokens_ref,
    expert_gain_ref,
    route_t_ref,
    route_weight_t_ref,
    gate_w_hbm,
    up_w_hbm,
    down_w_hbm,
    mixer_hbm,
    expert_out_ref,
    value,
    gate,
    out_weight,
    gate_w,
    up_w,
    down_w,
    halo_out,
    halo_in,
    padded,
    filtered,
    activated,
    outgoing,
    outgoing_wide,
    arrived,
    hidden,
    partial,
    half_in,
    pair_out,
    pair_in,
    summed,
    returned,
    mixer,
    weight_high,
    weight_low,
    load_sem,
    halo_sem,
    disp_send,
    disp_recv,
    wide_send,
    wide_recv,
    f1_send,
    f1_recv,
    f2_send,
    f2_recv,
    r1_send,
    r1_recv,
    r2_send,
    r2_recv,
    ret_send,
    ret_recv,
):
    i = lax.axis_index("ep")
    q = lax.axis_index("tp")
    q1 = q + 1 - 2 * lax.rem(q, 2)
    q2 = lax.rem(q + 2, 4)
    q3 = lax.rem(q1 + 2, 4)
    tokens, width = tokens_ref.shape
    cols = width // n_tp
    rows_all = n_ep * capacity
    group_rows = max(128, capacity)
    per_group = group_rows // capacity
    groups = rows_all // group_rows
    length, channels = value.shape
    lane_tiles = channels // LANES
    taps = taps_ref.shape[0]
    rim = halo_out.shape[0]
    first = 1 if per_group == 1 else 0
    near = 0
    paired = max(first, near)

    loads = [
        pltpu.make_async_copy(s, d, load_sem.at[n])
        for n, (s, d) in enumerate(
            (
                (gate_w_hbm.at[0], gate_w),
                (up_w_hbm.at[0], up_w),
                (down_w_hbm.at[0], down_w),
                (gate_hbm, gate),
                (value_hbm, value),
                (out_weight_hbm, out_weight),
            )
        )
    ]
    for load in loads:
        load.start()

    def peer(k):
        other, bit = 0, 1
        while bit < n_ep:
            other = other + bit * lax.rem(i // bit + k // bit, 2)
            bit *= 2
        return other

    def remote(src, dst, send, recv, ep, tp):
        return pltpu.make_async_remote_copy(
            src_ref=src,
            dst_ref=dst,
            send_sem=send,
            recv_sem=recv,
            device_id={"ep": ep, "tp": tp},
            device_id_type=pl.DeviceIdType.MESH,
        )

    def block(k):
        return pl.ds(pl.multiple_of(k * capacity, capacity), capacity)

    def group(g):
        return pl.ds(pl.multiple_of(g * group_rows, group_rows), group_rows)

    def dispatch(k):
        return remote(
            outgoing.at[block(k)],
            arrived.at[q, block(k)],
            disp_send.at[k],
            disp_recv.at[k],
            peer(k),
            q,
        )

    def dispatch_wide(k):
        return remote(
            outgoing_wide.at[block(k)],
            arrived.at[q2, block(k)],
            wide_send.at[k],
            wide_recv.at[k],
            peer(k),
            q,
        )

    def spread_pair(g):
        at = arrived.at[q, group(g)]
        return remote(at, at, f1_send.at[g], f1_recv.at[g], i, q2)

    def spread_core(g, n):
        at = arrived.at[q if n == 0 else q2, group(g)]
        return remote(at, at, f2_send.at[g, n], f2_recv.at[g, n], i, q1)

    def reduce_core(g, n):
        return remote(
            partial.at[q1 if n == 0 else q3, group(g)],
            half_in.at[n, group(g)],
            r1_send.at[g, n],
            r1_recv.at[g, n],
            i,
            q1,
        )

    def reduce_pair(g):
        return remote(
            pair_out.at[group(g)], pair_in.at[group(g)], r2_send.at[g], r2_recv.at[g], i, q2
        )

    def give_back(k):
        return remote(
            summed.at[block(k)],
            returned.at[block(k)],
            ret_send.at[k],
            ret_recv.at[k],
            peer(k),
            q,
        )

    here = i * n_tp + q
    following = lax.rem(here + 1, n_ep * n_tp)
    halo = remote(
        halo_out, halo_in, halo_sem.at[0], halo_sem.at[1], following // n_tp, lax.rem(following, n_tp)
    )

    def lower(a, b):
        return jnp.where(a < b, 1.0, 0.0).astype(bf16)

    side = (tokens, tokens)
    row_id = lax.broadcasted_iota(jnp.int32, side, 0)
    col_id = lax.broadcasted_iota(jnp.int32, side, 1)
    experts_t = lax.broadcasted_iota(jnp.int32, (n_ep, tokens), 0)
    picks_t = [route_t_ref[n : n + 1, :] for n in range(route_t_ref.shape[0])]
    hot_t = [jnp.where(experts_t == p, 1.0, 0.0) for p in picks_t]
    rank_t = dot(sum(hot_t).astype(bf16), lower(row_id, col_id))
    slot_rows = lax.broadcasted_iota(jnp.int32, (rows_all, tokens), 0).astype(f32)
    chosen = jnp.zeros((rows_all, tokens), f32)
    targets = []
    for p, h in zip(picks_t, hot_t):
        target = (jnp.bitwise_xor(p, i) * capacity).astype(f32) + jnp.sum(
            rank_t * h, 0, keepdims=True
        )
        targets.append(target)
        chosen = jnp.where(slot_rows == target, 1.0, chosen)

    x = tokens_ref[...].astype(f32)
    scale = lax.rsqrt(jnp.mean(x * x, 1, keepdims=True) + epsilon)
    chosen = chosen.astype(bf16)

    def columns(n):
        at = pl.ds(pl.multiple_of(n * cols, cols), cols)
        return (tokens_ref[:, at].astype(f32) * scale * expert_gain_ref[:, at]).astype(bf16)

    outgoing[...] = dot(chosen, columns(q)).astype(bf16)

    def start_dispatch(k, c):
        dispatch(k).start()
        return c

    lax.fori_loop(1, n_ep, start_dispatch, 0)
    if near:
        outgoing_wide[...] = dot(chosen[0 : near * capacity], columns(q2)).astype(bf16)
        for k in range(1, near):
            dispatch_wide(k).start()

    if first:
        for n in range(n_tp):
            arrived[n, 0:capacity] = dot(chosen[0:capacity], columns(n)).astype(bf16)
    else:
        arrived[q, 0:capacity] = outgoing[0:capacity]

    loads[3].wait()
    loads[4].wait()
    edge = pl.ds(length - rim, rim)
    halo_out[...] = (value[edge].astype(f32) * jax.nn.sigmoid(gate[edge].astype(f32))).astype(bf16)
    halo.start()

    def gate_tile(l, c):
        at = pl.ds(pl.multiple_of(l * LANES, LANES), LANES)
        padded[l, rim:] = (
            (value[:, at].astype(f32) * jax.nn.sigmoid(gate[:, at].astype(f32)))
            .astype(bf16)
            .astype(f32)
        )
        return c

    lax.fori_loop(0, lane_tiles, gate_tile, 0)
    for load in loads[:3]:
        load.wait()
    keep = jnp.where(here == 0, 0.0, 1.0).astype(f32)

    def conv_tile(l, c):
        at = pl.ds(pl.multiple_of(l * LANES, LANES), LANES)
        padded[l, 0:rim] = halo_in[:, at].astype(f32) * keep
        total = jnp.zeros((length, LANES), f32) + bias_ref[:, at]
        for j in range(taps):
            total = total + taps_ref[j : j + 1, at] * padded[l, pl.ds(rim - taps + 1 + j, length)]
        filtered[:, at] = total
        return c

    def norm_rows(r, c):
        at = pl.ds(pl.multiple_of(r * 32, 32), 32)
        f = filtered[at]
        centred = f - jnp.mean(f, 1, keepdims=True)
        variance = jnp.mean(centred * centred, 1, keepdims=True)
        v = centred * lax.rsqrt(variance + epsilon) * gain_ref[...] + shift_ref[...]
        activated[at] = (v * jax.nn.sigmoid(v)).astype(bf16)
        return c

    def project(n, c):
        at = pl.ds(pl.multiple_of(n * 256, 256), 256)
        mixer[:, at] = (dot(activated[...], out_weight[:, at]) + out_bias_ref[:, at]).astype(bf16)
        return c

    def experts_of(g):
        at = group(g)

        def unit(n, c):
            u_at = pl.ds(pl.multiple_of(n * 256, 256), 256)
            g_pre = jnp.zeros((group_rows, 256), f32)
            u_pre = jnp.zeros((group_rows, 256), f32)
            for s in range(n_tp):
                rows = arrived[s, at]
                k_at = pl.ds(s * cols, cols)
                g_pre = g_pre + dot(rows, gate_w[k_at, u_at])
                u_pre = u_pre + dot(rows, up_w[k_at, u_at])
            held = jnp.minimum(g_pre, clamp_limit)
            up = jnp.clip(u_pre, -clamp_limit, clamp_limit)
            hidden[:, u_at] = (held * jax.nn.sigmoid(swish_alpha * held) * (up + 1.0)).astype(bf16)
            return c

        lax.fori_loop(0, gate_w.shape[1] // 256, unit, 0)

        def down(s, c):
            at_cols = pl.ds(pl.multiple_of(s * cols, cols), cols)
            partial[s, at] = dot(hidden[...], down_w[:, at_cols]).astype(bf16)
            return c

        lax.fori_loop(0, n_tp, down, 0)

    def arrive(k, c):
        dispatch(k).wait_recv()
        return c

    def take_in(g):
        lax.fori_loop(jnp.maximum(g * per_group, 1), (g + 1) * per_group, arrive, 0)

        @pl.when(g >= near)
        def _():
            spread_pair(g).start()

        if near:

            @pl.when(g < near)
            def _():
                dispatch_wide(g).wait_recv()

    def give(k, c):
        give_back(k).start()
        return c

    mixer_store = pltpu.make_async_copy(mixer, mixer_hbm, load_sem.at[6])

    def step(t, c):
        @pl.when(jnp.logical_and(t >= 1 + first, t < groups + 1))
        def _():
            g = t - 1

            @pl.when(g >= paired)
            def _():
                spread_pair(g).wait_recv()

            spread_core(g, 0).start()
            spread_core(g, 1).start()

        @pl.when(t >= 3)
        def _():
            g = t - 3
            at = group(g)
            reduce_pair(g).wait_recv()
            summed[at] = (
                partial[q, at].astype(f32) + half_in[0, at].astype(f32) + pair_in[at].astype(f32)
            ).astype(bf16)
            lax.fori_loop(jnp.maximum(g * per_group, 1), (g + 1) * per_group, give, 0)

        @pl.when(t + 1 < groups)
        def _():
            take_in(t + 1)

        @pl.when(jnp.logical_and(t >= 1 + first, t < groups + 1))
        def _():
            spread_core(t - 1, 0).wait_recv()
            spread_core(t - 1, 1).wait_recv()

        @pl.when(t < groups + 1)
        def _():
            experts_of(t - 1)
            reduce_core(t - 1, 0).start()
            reduce_core(t - 1, 1).start()

        @pl.when(t == 1)
        def _():
            halo.wait_recv()

        @pl.when(t <= 4)
        def _():
            part = -(-lane_tiles // 4)
            lax.fori_loop((t - 1) * part, jnp.minimum(t * part, lane_tiles), conv_tile, 0)

        @pl.when(t == 5)
        def _():
            lax.fori_loop(0, length // 32, norm_rows, 0)

        @pl.when(t == 6)
        def _():
            loads[5].wait()
            lax.fori_loop(0, out_weight.shape[1] // 256, project, 0)
            mixer_store.start()

        @pl.when(t == 7)
        def _():
            weights = jnp.zeros((rows_all, tokens), f32)
            for n, target in enumerate(targets):
                weights = jnp.where(slot_rows == target, route_weight_t_ref[n : n + 1, :], weights)
            weights = weights.T
            high = weights.astype(bf16)
            weight_high[...] = high
            weight_low[...] = (weights - high.astype(f32)).astype(bf16)

        @pl.when(t < groups + 1)
        def _():
            at = group(t - 1)
            reduce_core(t - 1, 0).wait_recv()
            reduce_core(t - 1, 1).wait_recv()
            pair_out[at] = (partial[q2, at].astype(f32) + half_in[1, at].astype(f32)).astype(bf16)
            reduce_pair(t - 1).start()

        return c

    for g in range(first, 2):
        take_in(jnp.int32(g))
    lax.fori_loop(1, groups + 3, step, 0)
    returned[0:capacity] = summed[0:capacity]

    def came_back(k, c):
        give_back(k).wait_recv()
        return c

    lax.fori_loop(1, n_ep, came_back, 0)
    expert_out_ref[...] = (
        dot(weight_high[...], returned[...]) + dot(weight_low[...], returned[...])
    ).astype(bf16)

    halo.wait_send()
    mixer_store.wait()

    def sent(k, c):
        dispatch(k).wait_send()
        give_back(k).wait_send()
        return c

    lax.fori_loop(1, n_ep, sent, 0)

    def sent_group(g, c):
        reduce_pair(g).wait_send()
        for n in range(2):
            reduce_core(g, n).wait_send()
        return c

    lax.fori_loop(0, groups, sent_group, 0)

    def spread_sent(g, c):
        @pl.when(g >= paired)
        def _():
            spread_pair(g).wait_send()

        for n in range(2):
            spread_core(g, n).wait_send()
        return c

    lax.fori_loop(first, groups, spread_sent, 0)
    for k in range(1, near):
        dispatch_wide(k).wait_send()


def local(
    n_ep,
    n_tp,
    filter_value,
    filter_gate,
    filter_taps,
    filter_bias,
    norm_gain,
    norm_shift,
    out_weight,
    out_bias,
    expert_input,
    expert_gain,
    route_experts,
    route_weights,
    gate_weights,
    up_weights,
    down_weights,
):
    assert n_tp == 4 and n_ep & (n_ep - 1) == 0
    tokens, width = expert_input.shape
    capacity = 2 * tokens * route_experts.shape[1] // n_ep
    rows_all = n_ep * capacity
    group_rows = max(128, capacity)
    groups = rows_all // group_rows
    cols = width // n_tp
    length, channels = filter_value.shape
    units = gate_weights.shape[2]
    rim = -(-(filter_taps.shape[0] - 1) // 16) * 16
    vmem = pl.BlockSpec(memory_space=pltpu.VMEM)
    hbm = pl.BlockSpec(memory_space=pl.ANY)
    dma = pltpu.SemaphoreType.DMA
    return tuple(
        pl.pallas_call(
            functools.partial(kernel, n_ep, n_tp, capacity),
            out_shape=(
                jax.ShapeDtypeStruct((length, out_weight.shape[1]), bf16),
                jax.ShapeDtypeStruct((tokens, cols), bf16),
            ),
            in_specs=[hbm, hbm, vmem, vmem, vmem, vmem, hbm] + [vmem] * 5 + [hbm] * 3,
            out_specs=(hbm, vmem),
            scratch_shapes=[
                pltpu.VMEM((length, channels), bf16),
                pltpu.VMEM((length, channels), bf16),
                pltpu.VMEM(out_weight.shape, bf16),
                pltpu.VMEM((width, units), bf16),
                pltpu.VMEM((width, units), bf16),
                pltpu.VMEM((units, width), bf16),
                pltpu.VMEM((rim, channels), bf16),
                pltpu.VMEM((rim, channels), bf16),
                pltpu.VMEM((channels // LANES, rim + length, LANES), f32),
                pltpu.VMEM((length, channels), f32),
                pltpu.VMEM((length, channels), bf16),
                pltpu.VMEM((rows_all, cols), bf16),
                pltpu.VMEM((rows_all // 2, cols), bf16),
                pltpu.VMEM((n_tp, rows_all, cols), bf16),
                pltpu.VMEM((group_rows, units), bf16),
                pltpu.VMEM((n_tp, rows_all, cols), bf16),
                pltpu.VMEM((2, rows_all, cols), bf16),
                pltpu.VMEM((rows_all, cols), bf16),
                pltpu.VMEM((rows_all, cols), bf16),
                pltpu.VMEM((rows_all, cols), bf16),
                pltpu.VMEM((rows_all, cols), bf16),
                pltpu.VMEM((length, out_weight.shape[1]), bf16),
                pltpu.VMEM((tokens, rows_all), bf16),
                pltpu.VMEM((tokens, rows_all), bf16),
                dma((7,)),
                dma((2,)),
                dma((n_ep,)),
                dma((n_ep,)),
                dma((n_ep,)),
                dma((n_ep,)),
                dma((groups,)),
                dma((groups,)),
                dma((groups, 2)),
                dma((groups, 2)),
                dma((groups, 2)),
                dma((groups, 2)),
                dma((groups,)),
                dma((groups,)),
                dma((n_ep,)),
                dma((n_ep,)),
            ],
            compiler_params=pltpu.CompilerParams(
                has_side_effects=True, vmem_limit_bytes=60 * 1024 * 1024
            ),
            name="mixer_and_experts",
        )(
            filter_value,
            filter_gate,
            filter_taps,
            filter_bias[None],
            norm_gain[None],
            norm_shift[None],
            out_weight,
            out_bias[None],
            expert_input,
            expert_gain[None],
            route_experts.T,
            route_weights.T,
            gate_weights,
            up_weights,
            down_weights,
        )
    )


def solution(mesh):
    in_specs = (
        P(("ep", "tp"), None),
        P(("ep", "tp"), None),
        P(),
        P(),
        P(),
        P(),
        P(),
        P(),
        P("ep", None),
        P(),
        P("ep", None),
        P("ep", None),
        P("ep", None, "tp"),
        P("ep", None, "tp"),
        P("ep", "tp", None),
    )
    out_specs = (P(("ep", "tp"), None), P("ep", "tp"))
    body = functools.partial(local, mesh.shape["ep"], mesh.shape["tp"])
    return jax.shard_map(body, mesh=mesh, in_specs=in_specs, out_specs=out_specs, check_vma=False)
```

profile of v0, /device:TPU:14, one launch (start us, length us, event | category | flops | bytes accessed | tf_op | source)
XLA Modules:
  0.0 89.0 jit_solution(16986298920917755092)
XLA Ops:
  0.6 85.3 %mixer_and_experts.1 = (bf16[256,2048]{1,0:T(8,128)(2,1)}, bf16[256,512]{1,0:T(8,128)(2,1)}) custom-call(bf16[256,1024]{1,0:T(8,128)(2,1)} %value_hbm.1, bf16[256,1024]{1,0:T(8,128)(2,1)} %gate_hbm.1, f32[31,1024]{1,0:T(8,128)} %taps_ref.1, f32[1,1024]{1,0:T(1,128)} %bitcast.9, f32[1,1024]{1,0:T(1,128)} %bitcast.10, f32[1,1024]{1,0:T(1,128)} %bitcast.11, ...), custom_call_target="tpu_custom_call" | custom-call | tf_op jit(solution)/shard_map/mixer_and_experts/pallas_call | solution.py:494
  86.0 0.0 copy-start
  86.0 2.3 %copy.19 = bf16[256,2048]{1,0:T(8,128)(2,1)} copy(bf16[256,2048]{1,0:T(8,128)(2,1)} %get-tuple-element.4) | data formatting | bytes 2097152
  88.3 0.0 copy-done
  88.3 0.7 copy.20
Async XLA Ops:
  86.0 2.4 %copy-start = (bf16[256,512]{1,0:T(8,128)(2,1)S(1)}, bf16[256,512]{1,0:T(8,128)(2,1)}, u32[]{:S(2)}) copy-start(bf16[256,512]{1,0:T(8,128)(2,1)} %get-tuple-element.5) | copy-start | bytes 786436
where the time goes:
time: 89.2 us; the launch traced here: 89 us
  Pallas kernels  85.3 us (96%)
  local copies, waits for them, and re-layouts  3.05 us (3%)
    pallas_call x1, Pallas kernels, local(): pl.pallas_call(functools.partial(kernel, n_ep, n_tp, capacity), out_shape...  85.3 us
    unnamed x4, local copies, waits for them, and re-layouts  3.05 us

commit v1 on v0

v1 whole, which is shorter than its diff:
```python
import functools

import jax
import jax.numpy as jnp
from jax import lax
from jax.experimental import pallas as pl
from jax.experimental.pallas import tpu as pltpu
from jax.sharding import PartitionSpec as P

epsilon = 1e-06
clamp_limit = 7.0
swish_alpha = 1.702
LANES = 128
SCHEDULE = (
    "C0 F0 D0 S1",
    "F1 F2 F3 A1",
    "A2 S2 C1 F4",
    "D1 E0 B2 F5",
    "A4 C2 S3 A3",
    "F6 D2 C3 B4",
    "E1 D3 C4 A6",
    "E2 D4 A7 A5",
    "C5 B6 F7 C6",
    "E4 D6 B7 E3",
    "C7 E6 D7 D5",
    "E7 E5",
)
f32 = jnp.float32
bf16 = jnp.bfloat16


def dot(a, b):
    return jnp.dot(a, b, preferred_element_type=f32)


def kernel(
    n_ep,
    n_tp,
    capacity,
    value_hbm,
    gate_hbm,
    taps_hbm,
    bias_hbm,
    gain_hbm,
    shift_hbm,
    out_weight_hbm,
    out_bias_hbm,
    tokens_hbm,
    expert_gain_hbm,
    route_t_hbm,
    route_weight_t_hbm,
    gate_w_hbm,
    up_w_hbm,
    down_w_hbm,
    mixer,
    expert_out_ref,
    value,
    gate,
    taps_ref,
    bias_ref,
    gain_ref,
    shift_ref,
    out_weight,
    out_bias_ref,
    tokens_ref,
    expert_gain_ref,
    route_t_ref,
    route_weight_t_ref,
    gate_w,
    up_w,
    down_w,
    halo_out,
    halo_in,
    padded,
    filtered,
    activated,
    outgoing,
    outgoing_wide,
    arrived,
    hidden,
    partial,
    half_in,
    pair_out,
    pair_in,
    summed,
    returned,
    weight_high,
    weight_low,
    load_sem,
    halo_sem,
    disp_send,
    disp_recv,
    wide_send,
    wide_recv,
    f1_send,
    f1_recv,
    f2_send,
    f2_recv,
    r1_send,
    r1_recv,
    r2_send,
    r2_recv,
    ret_send,
    ret_recv,
):
    i = lax.axis_index("ep")
    q = lax.axis_index("tp")
    q1 = q + 1 - 2 * lax.rem(q, 2)
    q2 = lax.rem(q + 2, 4)
    q3 = lax.rem(q1 + 2, 4)
    tokens, width = tokens_ref.shape
    cols = width // n_tp
    rows_all = n_ep * capacity
    group_rows = max(128, capacity)
    per_group = group_rows // capacity
    groups = rows_all // group_rows
    length, channels = value.shape
    lane_tiles = channels // LANES
    taps = taps_ref.shape[0]
    rim = halo_out.shape[0]
    single = per_group == 1
    near = n_ep // 2 if single else 0
    here = i * n_tp + q
    last = n_ep * n_tp - 1
    following = lax.rem(here + 1, n_ep * n_tp)

    def peer(k):
        other, bit = 0, 1
        while bit < n_ep:
            other = other + bit * lax.rem(i // bit + k // bit, 2)
            bit *= 2
        return other

    barrier = pltpu.get_barrier_semaphore()

    def greet(ep, tp):
        pl.semaphore_signal(
            barrier,
            inc=1,
            device_id={"ep": ep, "tp": tp},
            device_id_type=pl.DeviceIdType.MESH,
        )

    def greet_peer(k, c):
        greet(peer(k), q)
        return c

    lax.fori_loop(1, n_ep, greet_peer, 0)
    greet(i, q1)
    greet(i, q2)

    @pl.when(here > 0)
    def _():
        greet((here - 1) // n_tp, lax.rem(here - 1, n_tp))

    copies = (
        ("route", route_t_hbm, route_t_ref),
        ("tokens", tokens_hbm, tokens_ref),
        ("expert_gain", expert_gain_hbm, expert_gain_ref),
        ("value", value_hbm, value),
        ("gate", gate_hbm, gate),
        ("taps", taps_hbm, taps_ref),
        ("bias", bias_hbm, bias_ref),
        ("gain", gain_hbm, gain_ref),
        ("shift", shift_hbm, shift_ref),
        ("out_bias", out_bias_hbm, out_bias_ref),
        ("weight_t", route_weight_t_hbm, route_weight_t_ref),
        ("gate_w", gate_w_hbm.at[0], gate_w),
        ("up_w", up_w_hbm.at[0], up_w),
        ("down_w", down_w_hbm.at[0], down_w),
        ("out_weight", out_weight_hbm, out_weight),
    )
    names = [name for name, _, _ in copies]
    loads = {
        name: pltpu.make_async_copy(s, d, load_sem.at[n])
        for n, (name, s, d) in enumerate(copies)
    }
    for name in names[:11]:
        loads[name].start()

    def remote(src, dst, send, recv, ep, tp):
        return pltpu.make_async_remote_copy(
            src_ref=src,
            dst_ref=dst,
            send_sem=send,
            recv_sem=recv,
            device_id={"ep": ep, "tp": tp},
            device_id_type=pl.DeviceIdType.MESH,
        )

    def block(k):
        return pl.ds(pl.multiple_of(k * capacity, capacity), capacity)

    def group(g):
        return pl.ds(pl.multiple_of(g * group_rows, group_rows), group_rows)

    def dispatch(k):
        return remote(
            outgoing.at[block(k)],
            arrived.at[q, block(k)],
            disp_send.at[k],
            disp_recv.at[k],
            peer(k),
            q,
        )

    def dispatch_wide(k):
        return remote(
            outgoing_wide.at[block(k)],
            arrived.at[q2, block(k)],
            wide_send.at[k],
            wide_recv.at[k],
            peer(k),
            q,
        )

    def spread_pair(g):
        at = arrived.at[q, group(g)]
        return remote(at, at, f1_send.at[g], f1_recv.at[g], i, q2)

    def spread_core(g, n):
        at = arrived.at[q if n == 0 else q2, group(g)]
        return remote(at, at, f2_send.at[g, n], f2_recv.at[g, n], i, q1)

    def reduce_core(g, n):
        return remote(
            partial.at[q1 if n == 0 else q3, group(g)],
            half_in.at[n, group(g)],
            r1_send.at[g, n],
            r1_recv.at[g, n],
            i,
            q1,
        )

    def reduce_pair(g):
        return remote(
            pair_out.at[group(g)], pair_in.at[group(g)], r2_send.at[g], r2_recv.at[g], i, q2
        )

    def give_back(k):
        return remote(
            summed.at[block(k)],
            returned.at[block(k)],
            ret_send.at[k],
            ret_recv.at[k],
            peer(k),
            q,
        )

    halo = remote(
        halo_out, halo_in, halo_sem.at[0], halo_sem.at[1], following // n_tp, lax.rem(following, n_tp)
    )

    def lower(a, b):
        return jnp.where(a < b, 1.0, 0.0).astype(bf16)

    side = (tokens, tokens)
    row_id = lax.broadcasted_iota(jnp.int32, side, 0)
    col_id = lax.broadcasted_iota(jnp.int32, side, 1)
    experts_t = lax.broadcasted_iota(jnp.int32, (n_ep, tokens), 0)
    loads["route"].wait()
    picks_t = [route_t_ref[n : n + 1, :] for n in range(route_t_ref.shape[0])]
    hot_t = [jnp.where(experts_t == p, 1.0, 0.0) for p in picks_t]
    rank_t = dot(sum(hot_t).astype(bf16), lower(row_id, col_id))
    slot_rows = lax.broadcasted_iota(jnp.int32, (rows_all, tokens), 0).astype(f32)
    chosen = jnp.zeros((rows_all, tokens), f32)
    targets = []
    for p, h in zip(picks_t, hot_t):
        target = (jnp.bitwise_xor(p, i) * capacity).astype(f32) + jnp.sum(
            rank_t * h, 0, keepdims=True
        )
        targets.append(target)
        chosen = jnp.where(slot_rows == target, 1.0, chosen)

    with jax.named_scope("w_tok"):
        loads["tokens"].wait()
    for name in names[11:]:
        loads[name].start()
    x = tokens_ref[...].astype(f32)
    scale = lax.rsqrt(jnp.mean(x * x, 1, keepdims=True) + epsilon)
    chosen = chosen.astype(bf16)
    loads["expert_gain"].wait()

    def columns(n):
        at = pl.ds(pl.multiple_of(n * cols, cols), cols)
        return (tokens_ref[:, at].astype(f32) * scale * expert_gain_ref[:, at]).astype(bf16)

    with jax.named_scope("select"):
        outgoing[...] = dot(chosen, columns(q)).astype(bf16)
        if near:
            outgoing_wide[...] = dot(chosen[0 : near * capacity], columns(q2)).astype(bf16)
    loads["value"].wait()
    loads["gate"].wait()
    edge = pl.ds(length - rim, rim)
    halo_out[...] = (value[edge].astype(f32) * jax.nn.sigmoid(gate[edge].astype(f32))).astype(bf16)

    with jax.named_scope("w_barrier"):
        pl.semaphore_wait(barrier, n_ep + 2 - jnp.where(here == last, 1, 0))

    @pl.when(here < last)
    def _():
        halo.start()

    @pl.when(here == 0)
    def _():
        halo_in[...] = jnp.zeros_like(halo_in)

    if single and n_ep == 8:
        staged = ((1, -1, 4, 2), (5, -2), (6, 3), (7, -3))
    else:
        staged = (range(1, n_ep),)

    def send(n):
        for k in staged[n] if n < len(staged) else ():
            (dispatch(k) if k > 0 else dispatch_wide(-k)).start()

    with jax.named_scope("wide"):
        send(0)
        if single:
            for n in range(n_tp):
                arrived[n, 0:capacity] = dot(chosen[0:capacity], columns(n)).astype(bf16)
        else:
            arrived[q, 0:capacity] = outgoing[0:capacity]

    def gate_tile(l, c):
        at = pl.ds(pl.multiple_of(l * LANES, LANES), LANES)
        padded[l, rim:] = (
            (value[:, at].astype(f32) * jax.nn.sigmoid(gate[:, at].astype(f32)))
            .astype(bf16)
            .astype(f32)
        )
        return c

    def conv_tile(l, c):
        at = pl.ds(pl.multiple_of(l * LANES, LANES), LANES)
        padded[l, 0:rim] = halo_in[:, at].astype(f32)
        total = jnp.zeros((length, LANES), f32) + bias_ref[:, at]
        for j in range(taps):
            total = total + taps_ref[j : j + 1, at] * padded[l, pl.ds(rim - taps + 1 + j, length)]
        filtered[:, at] = total
        return c

    def norm_rows(r, c):
        at = pl.ds(pl.multiple_of(r * 32, 32), 32)
        f = filtered[at]
        centred = f - jnp.mean(f, 1, keepdims=True)
        variance = jnp.mean(centred * centred, 1, keepdims=True)
        v = centred * lax.rsqrt(variance + epsilon) * gain_ref[...] + shift_ref[...]
        activated[at] = (v * jax.nn.sigmoid(v)).astype(bf16)
        return c

    def project(n, c):
        at = pl.ds(pl.multiple_of(n * 256, 256), 256)
        mixer[:, at] = (dot(activated[...], out_weight[:, at]) + out_bias_ref[:, at]).astype(bf16)
        return c

    def experts_of(gs):
        ats = [group(g) for g in gs]
        held_rows = pl.ds(0, len(gs) * group_rows)

        def unit(n, c):
            u_at = pl.ds(pl.multiple_of(n * 256, 256), 256)
            rows = jnp.concatenate(
                [jnp.concatenate([arrived[s, at] for s in range(n_tp)], 1) for at in ats], 0
            )
            g_pre = dot(rows, gate_w[:, u_at])
            u_pre = dot(rows, up_w[:, u_at])
            held = jnp.minimum(g_pre, clamp_limit)
            up = jnp.clip(u_pre, -clamp_limit, clamp_limit)
            hidden[held_rows, u_at] = (held * jax.nn.sigmoid(swish_alpha * held) * (up + 1.0)).astype(bf16)
            return c

        lax.fori_loop(0, gate_w.shape[1] // 256, unit, 0)

        def down(s, c):
            at_cols = pl.ds(pl.multiple_of(s * cols, cols), cols)
            part = dot(hidden[held_rows, :], down_w[:, at_cols]).astype(bf16)
            for n, at in enumerate(ats):
                partial[s, at] = part[n * group_rows : (n + 1) * group_rows]
            return c

        lax.fori_loop(0, n_tp, down, 0)

    def arrive(k, c):
        dispatch(k).wait_recv()
        return c

    def give(k, c):
        give_back(k).start()
        return c

    if single and n_ep == 8:
        order = [0, 1, 4, 2, 5, 3, 6, 7]
    else:
        order = list(range(groups))
    wide = [g < near for g in order]
    order = [jnp.int32(g) for g in order]

    def take(s):
        g = order[s]
        if single and s == 0:
            return
        with jax.named_scope(f"A{s}"):
            lax.fori_loop(jnp.maximum(g * per_group, 1), (g + 1) * per_group, arrive, 0)
            if wide[s]:
                dispatch_wide(g).wait_recv()
            else:
                spread_pair(g).start()
            spread_core(g, 0).start()
            if wide[s]:
                spread_core(g, 1).start()

    def relay(s):
        g = order[s]
        if wide[s]:
            return
        with jax.named_scope(f"B{s}"):
            spread_pair(g).wait_recv()
            spread_core(g, 1).start()

    def compute(*steps):
        for s in steps:
            if not (single and s == 0):
                with jax.named_scope(f"Cw{s}"):
                    spread_core(order[s], 0).wait_recv()
                    spread_core(order[s], 1).wait_recv()
        with jax.named_scope(f"C{steps}"):
            experts_of([order[s] for s in steps])
        for s in steps:
            reduce_core(order[s], 0).start()
            reduce_core(order[s], 1).start()

    def halve(s):
        g = order[s]
        at = group(g)
        with jax.named_scope(f"D{s}"):
            reduce_core(g, 0).wait_recv()
            reduce_core(g, 1).wait_recv()
            pair_out[at] = (partial[q2, at].astype(f32) + half_in[1, at].astype(f32)).astype(bf16)
            reduce_pair(g).start()

    def finish(s):
        g = order[s]
        at = group(g)
        with jax.named_scope(f"E{s}"):
            reduce_pair(g).wait_recv()
            summed[at] = (
                partial[q, at].astype(f32) + half_in[0, at].astype(f32) + pair_in[at].astype(f32)
            ).astype(bf16)
            lax.fori_loop(jnp.maximum(g * per_group, 1), (g + 1) * per_group, give, 0)

    def mixer_gate():
        lax.fori_loop(0, lane_tiles, gate_tile, 0)

    def mixer_halo():
        for name in ("taps", "bias", "gain", "shift"):
            loads[name].wait()

        @pl.when(here > 0)
        def _():
            halo.wait_recv()

    def mixer_conv(n):
        lax.fori_loop(n * lane_tiles // 2, (n + 1) * lane_tiles // 2, conv_tile, 0)

    def mixer_norm():
        lax.fori_loop(0, length // 32, norm_rows, 0)

    def mixer_project(n):
        if n == 0:
            loads["out_weight"].wait()
            loads["out_bias"].wait()
        tiles = out_weight.shape[1] // 256
        lax.fori_loop(n * tiles // 2, (n + 1) * tiles // 2, project, 0)

    def weigh():
        loads["weight_t"].wait()
        weights = jnp.zeros((rows_all, tokens), f32)
        for n, target in enumerate(targets):
            weights = jnp.where(slot_rows == target, route_weight_t_ref[n : n + 1, :], weights)
        weights = weights.T
        high = weights.astype(bf16)
        weight_high[...] = high
        weight_low[...] = (weights - high.astype(f32)).astype(bf16)

    fillers = [
        mixer_gate,
        mixer_halo,
        functools.partial(mixer_conv, 0),
        functools.partial(mixer_conv, 1),
        mixer_norm,
        functools.partial(mixer_project, 0),
        functools.partial(mixer_project, 1),
        weigh,
    ]

    def fill(n):
        with jax.named_scope(f"F{n}"):
            fillers[n]()

    for name in ("gate_w", "up_w", "down_w"):
        loads[name].wait()
    stages = {"A": take, "B": relay, "S": send, "C": compute, "D": halve, "E": finish, "F": fill}
    for word in " ".join(SCHEDULE).split():
        stages[word[0]](*[int(n) for n in word[1:].split("+")])
    returned[0:capacity] = summed[0:capacity]

    def came_back(k, c):
        give_back(k).wait_recv()
        return c

    with jax.named_scope("w_ret"):
        lax.fori_loop(1, n_ep, came_back, 0)
    with jax.named_scope("final"):
        expert_out_ref[...] = (
            dot(weight_high[...], returned[...]) + dot(weight_low[...], returned[...])
        ).astype(bf16)

    @pl.when(here < last)
    def _():
        halo.wait_send()

    def sent(k, c):
        dispatch(k).wait_send()
        give_back(k).wait_send()
        return c

    with jax.named_scope("w_sent"):
        lax.fori_loop(1, n_ep, sent, 0)

    def sent_group(g, c):
        reduce_pair(g).wait_send()
        for n in range(2):
            reduce_core(g, n).wait_send()
        return c

    lax.fori_loop(0, groups, sent_group, 0)

    def spread_sent(g, c):
        if near == 0:
            spread_pair(g).wait_send()
        for n in range(2):
            spread_core(g, n).wait_send()
        return c

    lax.fori_loop(1 if single else 0, groups, spread_sent, 0)
    if near:
        for g in range(near, groups):
            spread_pair(g).wait_send()
    for k in range(1, near):
        dispatch_wide(k).wait_send()


def local(
    n_ep,
    n_tp,
    filter_value,
    filter_gate,
    filter_taps,
    filter_bias,
    norm_gain,
    norm_shift,
    out_weight,
    out_bias,
    expert_input,
    expert_gain,
    route_experts,
    route_weights,
    gate_weights,
    up_weights,
    down_weights,
):
    assert n_tp == 4 and n_ep & (n_ep - 1) == 0
    tokens, width = expert_input.shape
    capacity = 2 * tokens * route_experts.shape[1] // n_ep
    rows_all = n_ep * capacity
    group_rows = max(128, capacity)
    groups = rows_all // group_rows
    cols = width // n_tp
    length, channels = filter_value.shape
    units = gate_weights.shape[2]
    rim = -(-(filter_taps.shape[0] - 1) // 16) * 16
    vmem = pl.BlockSpec(memory_space=pltpu.VMEM)
    hbm = pl.BlockSpec(memory_space=pltpu.HBM)
    dma = pltpu.SemaphoreType.DMA
    operands = (
        filter_value,
        filter_gate,
        filter_taps,
        filter_bias[None],
        norm_gain[None],
        norm_shift[None],
        out_weight,
        out_bias[None],
        expert_input,
        expert_gain[None],
        route_experts.T,
        route_weights.T,
    )
    inputs = [
        pltpu.with_memory_space_constraint(a, pltpu.HBM)
        for a in operands + (gate_weights, up_weights, down_weights)
    ]
    return tuple(
        pl.pallas_call(
            functools.partial(kernel, n_ep, n_tp, capacity),
            out_shape=(
                jax.ShapeDtypeStruct((length, out_weight.shape[1]), bf16),
                jax.ShapeDtypeStruct((tokens, cols), bf16),
            ),
            in_specs=[hbm] * 15,
            out_specs=(vmem, vmem),
            scratch_shapes=[pltpu.VMEM(a.shape, a.dtype) for a in operands]
            + [
                pltpu.VMEM((width, units), bf16),
                pltpu.VMEM((width, units), bf16),
                pltpu.VMEM((units, width), bf16),
                pltpu.VMEM((rim, channels), bf16),
                pltpu.VMEM((rim, channels), bf16),
                pltpu.VMEM((channels // LANES, rim + length, LANES), f32),
                pltpu.VMEM((length, channels), f32),
                pltpu.VMEM((length, channels), bf16),
                pltpu.VMEM((rows_all, cols), bf16),
                pltpu.VMEM((rows_all // 2, cols), bf16),
                pltpu.VMEM((n_tp, rows_all, cols), bf16),
                pltpu.VMEM((2 * group_rows, units), bf16),
                pltpu.VMEM((n_tp, rows_all, cols), bf16),
                pltpu.VMEM((2, rows_all, cols), bf16),
                pltpu.VMEM((rows_all, cols), bf16),
                pltpu.VMEM((rows_all, cols), bf16),
                pltpu.VMEM((rows_all, cols), bf16),
                pltpu.VMEM((rows_all, cols), bf16),
                pltpu.VMEM((tokens, rows_all), bf16),
                pltpu.VMEM((tokens, rows_all), bf16),
                dma((15,)),
                dma((2,)),
                dma((n_ep,)),
                dma((n_ep,)),
                dma((n_ep,)),
                dma((n_ep,)),
                dma((groups,)),
                dma((groups,)),
                dma((groups, 2)),
                dma((groups, 2)),
                dma((groups, 2)),
                dma((groups, 2)),
                dma((groups,)),
                dma((groups,)),
                dma((n_ep,)),
                dma((n_ep,)),
            ],
            compiler_params=pltpu.CompilerParams(
                has_side_effects=True, collective_id=0, vmem_limit_bytes=44 * 1024 * 1024
            ),
            name="mixer_and_experts",
        )(*inputs)
    )


def solution(mesh):
    in_specs = (
        P(("ep", "tp"), None),
        P(("ep", "tp"), None),
        P(),
        P(),
        P(),
        P(),
        P(),
        P(),
        P("ep", None),
        P(),
        P("ep", None),
        P("ep", None),
        P("ep", None, "tp"),
        P("ep", None, "tp"),
        P("ep", "tp", None),
    )
    out_specs = (P(("ep", "tp"), None), P("ep", "tp"))
    body = functools.partial(local, mesh.shape["ep"], mesh.shape["tp"])
    return jax.shard_map(body, mesh=mesh, in_specs=in_specs, out_specs=out_specs, check_vma=False)
```

time: 89.2 us -> 63.8 us (0.72)
  the two profiles are of different devices: /device:TPU:14 before, /device:TPU:0 now
where the time goes in v1:
time: 63.8 us; the launch traced here: 63.2 us
  Pallas kernels  60.8 us (95%)
  local copies, waits for them, and re-layouts  1.67 us (3%)
  between operations  0.64 us (1%)
    pallas_call x1, Pallas kernels, local(): pl.pallas_call(functools.partial(kernel, n_ep, n_tp, capacity), out_shape...  60.8 us
    unnamed x2, local copies, waits for them, and re-layouts  1.67 us

profile of v1, /device:TPU:0, one launch (start us, length us, event | category | flops | bytes accessed | tf_op | source)
XLA Modules:
  0.0 63.2 jit_solution(8809873678484283163)
XLA Ops:
  0.6 60.8 %mixer_and_experts.1 = (bf16[256,2048]{1,0:T(8,128)(2,1)S(1)}, bf16[256,512]{1,0:T(8,128)(2,1)S(1)}) custom-call(bf16[256,1024]{1,0:T(8,128)(2,1)} %value_hbm.1, bf16[256,1024]{1,0:T(8,128)(2,1)} %gate_hbm.1, f32[31,1024]{1,0:T(8,128)} %taps_hbm.1, f32[1,1024]{1,0:T(1,128)} %bitcast.9, f32[1,1024]{1,0:T(1,128)} %bitcast.10, f32[1,1024]{1,0:T(1,128)} %bitcast.11, ...), custom_call_target="tpu_custom_call" | custom-call | tf_op jit(solution)/shard_map/mixer_and_experts/pallas_call | solution.py:605
  61.5 1.0 %copy.19 = bf16[256,2048]{1,0:T(8,128)(2,1)} copy(bf16[256,2048]{1,0:T(8,128)(2,1)S(1)} %get-tuple-element.4) | data formatting | bytes 2097152
  62.5 0.7 %copy.20 = bf16[256,512]{1,0:T(8,128)(2,1)} copy(bf16[256,512]{1,0:T(8,128)(2,1)S(1)} %get-tuple-element.5) | data formatting | bytes 524288

commit v2 on v1

--- a/solution.py
+++ b/solution.py
@@ -13,16 +13,16 @@
 LANES = 128
 SCHEDULE = (
     "C0 F0 D0 S1",
-    "F1 F2 F3 A1",
+    "F1 F2 A1 F3",
     "A2 S2 C1 F4",
-    "D1 E0 B2 F5",
-    "A4 C2 S3 A3",
-    "F6 D2 C3 B4",
-    "E1 D3 C4 A6",
-    "E2 D4 A7 A5",
-    "C5 B6 F7 C6",
-    "E4 D6 B7 E3",
-    "C7 E6 D7 D5",
+    "D1 S3 E0 B2",
+    "F5 A4 C2 A3",
+    "F6 D2 B4 C3",
+    "A6 C4 E2 E1",
+    "D4 F7 B6 A5",
+    "C5 A7 C6 E4",
+    "D6 D3 B7 C7",
+    "E6 D7 D5 E3",
     "E7 E5",
 )
 f32 = jnp.float32
@@ -86,6 +86,7 @@
     returned,
     weight_high,
     weight_low,
+    expert_sum,
     load_sem,
     halo_sem,
     disp_send,
@@ -192,13 +193,13 @@
         return pl.ds(pl.multiple_of(k * capacity, capacity), capacity)
 
     def group(g):
-        return pl.ds(pl.multiple_of(g * group_rows, group_rows), group_rows)
+        return pl.ds(g * group_rows, group_rows)
 
     def dispatch(k):
         return remote(
             outgoing.at[block(k)],
             arrived.at[q, block(k)],
-            disp_send.at[k],
+            disp_send,
             disp_recv.at[k],
             peer(k),
             q,
@@ -208,40 +209,48 @@
         return remote(
             outgoing_wide.at[block(k)],
             arrived.at[q2, block(k)],
-            wide_send.at[k],
-            wide_recv.at[k],
+            wide_send,
+            wide_recv.at[k - 1],
             peer(k),
             q,
         )
 
     def spread_pair(g):
         at = arrived.at[q, group(g)]
-        return remote(at, at, f1_send.at[g], f1_recv.at[g], i, q2)
+        return remote(at, at, f1_send, f1_recv.at[g - near], i, q2)
 
     def spread_core(g, n):
         at = arrived.at[q if n == 0 else q2, group(g)]
-        return remote(at, at, f2_send.at[g, n], f2_recv.at[g, n], i, q1)
+        return remote(at, at, f2_send, f2_recv.at[g], i, q1)
 
     def reduce_core(g, n):
         return remote(
             partial.at[q1 if n == 0 else q3, group(g)],
             half_in.at[n, group(g)],
-            r1_send.at[g, n],
-            r1_recv.at[g, n],
+            r1_send,
+            r1_recv.at[g],
             i,
             q1,
         )
 
     def reduce_pair(g):
         return remote(
-            pair_out.at[group(g)], pair_in.at[group(g)], r2_send.at[g], r2_recv.at[g], i, q2
-        )
+            pair_out.at[group(g)], pair_in.at[group(g)], r2_send, r2_recv.at[g], i, q2
+        )
+
+    def two_halves(send, recv, rows):
+        at = half_in.at[:, pl.ds(0, rows)]
+        return remote(at, at, send, recv, i, q1)
+
+    def one_piece(send, rows):
+        at = pair_in.at[pl.ds(0, rows)]
+        return remote(at, at, send, r2_recv.at[0], i, q2)
 
     def give_back(k):
         return remote(
             summed.at[block(k)],
             returned.at[block(k)],
-            ret_send.at[k],
+            ret_send,
             ret_recv.at[k],
             peer(k),
             q,
@@ -316,6 +325,7 @@
 
     with jax.named_scope("wide"):
         send(0)
+    with jax.named_scope("own"):
         if single:
             for n in range(n_tp):
                 arrived[n, 0:capacity] = dot(chosen[0:capacity], columns(n)).astype(bf16)
@@ -394,7 +404,6 @@
     else:
         order = list(range(groups))
     wide = [g < near for g in order]
-    order = [jnp.int32(g) for g in order]
 
     def take(s):
         g = order[s]
@@ -422,8 +431,7 @@
         for s in steps:
             if not (single and s == 0):
                 with jax.named_scope(f"Cw{s}"):
-                    spread_core(order[s], 0).wait_recv()
-                    spread_core(order[s], 1).wait_recv()
+                    two_halves(f2_send, f2_recv.at[order[s]], group_rows).wait_recv()
         with jax.named_scope(f"C{steps}"):
             experts_of([order[s] for s in steps])
         for s in steps:
@@ -434,8 +442,7 @@
         g = order[s]
         at = group(g)
         with jax.named_scope(f"D{s}"):
-            reduce_core(g, 0).wait_recv()
-            reduce_core(g, 1).wait_recv()
+            two_halves(r1_send, r1_recv.at[g], group_rows).wait_recv()
             pair_out[at] = (partial[q2, at].astype(f32) + half_in[1, at].astype(f32)).astype(bf16)
             reduce_pair(g).start()
 
@@ -509,46 +516,49 @@
         give_back(k).wait_recv()
         return c
 
+    def weighted(low, high):
+        at = pl.ds(low * capacity, (high - low) * capacity)
+        return dot(weight_high[:, at], returned[at]) + dot(weight_low[:, at], returned[at])
+
     with jax.named_scope("w_ret"):
-        lax.fori_loop(1, n_ep, came_back, 0)
+        if single:
+            final = order[-1]
+            lax.fori_loop(1, final, came_back, 0)
+            expert_sum[...] = weighted(0, final)
+            came_back(final, 0)
+        else:
+            lax.fori_loop(1, n_ep, came_back, 0)
     with jax.named_scope("final"):
-        expert_out_ref[...] = (
-            dot(weight_high[...], returned[...]) + dot(weight_low[...], returned[...])
-        ).astype(bf16)
+        if single:
+            expert_out_ref[...] = (expert_sum[...] + weighted(final, n_ep)).astype(bf16)
+        else:
+            expert_out_ref[...] = weighted(0, n_ep).astype(bf16)
 
     @pl.when(here < last)
     def _():
         halo.wait_send()
 
-    def sent(k, c):
-        dispatch(k).wait_send()
-        give_back(k).wait_send()
-        return c
-
+    lead = group_rows if single else 0
     with jax.named_scope("w_sent"):
-        lax.fori_loop(1, n_ep, sent, 0)
-
-    def sent_group(g, c):
-        reduce_pair(g).wait_send()
-        for n in range(2):
-            reduce_core(g, n).wait_send()
-        return c
-
-    lax.fori_loop(0, groups, sent_group, 0)
-
-    def spread_sent(g, c):
-        if near == 0:
-            spread_pair(g).wait_send()
-        for n in range(2):
-            spread_core(g, n).wait_send()
-        return c
-
-    lax.fori_loop(1 if single else 0, groups, spread_sent, 0)
-    if near:
-        for g in range(near, groups):
-            spread_pair(g).wait_send()
-    for k in range(1, near):
-        dispatch_wide(k).wait_send()
+        one_piece(disp_send, rows_all - capacity).wait_send()
+        one_piece(ret_send, rows_all - capacity).wait_send()
+        one_piece(r2_send, rows_all).wait_send()
+        one_piece(f1_send, rows_all - near * group_rows).wait_send()
+        two_halves(r1_send, r1_recv.at[0], rows_all).wait_send()
+        two_halves(f2_send, f2_recv.at[0], rows_all - lead).wait_send()
+        if near:
+            one_piece(wide_send, (near - 1) * capacity).wait_send()
+
+
+def publish(mixer, expert, mixer_hbm, expert_hbm, sems):
+    copies = [
+        pltpu.make_async_copy(mixer, mixer_hbm, sems.at[0]),
+        pltpu.make_async_copy(expert, expert_hbm, sems.at[1]),
+    ]
+    for copy in copies:
+        copy.start()
+    for copy in copies:
+        copy.wait()
 
 
 def local(
@@ -601,13 +611,14 @@
         pltpu.with_memory_space_constraint(a, pltpu.HBM)
         for a in operands + (gate_weights, up_weights, down_weights)
     ]
-    return tuple(
+    results = (
+        jax.ShapeDtypeStruct((length, out_weight.shape[1]), bf16),
+        jax.ShapeDtypeStruct((tokens, cols), bf16),
+    )
+    mixed, expert_out = (
         pl.pallas_call(
             functools.partial(kernel, n_ep, n_tp, capacity),
-            out_shape=(
-                jax.ShapeDtypeStruct((length, out_weight.shape[1]), bf16),
-                jax.ShapeDtypeStruct((tokens, cols), bf16),
-            ),
+            out_shape=results,
             in_specs=[hbm] * 15,
             out_specs=(vmem, vmem),
             scratch_shapes=[pltpu.VMEM(a.shape, a.dtype) for a in operands]
@@ -632,21 +643,22 @@
                 pltpu.VMEM((rows_all, cols), bf16),
                 pltpu.VMEM((tokens, rows_all), bf16),
                 pltpu.VMEM((tokens, rows_all), bf16),
+                pltpu.VMEM((tokens, cols), f32),
                 dma((15,)),
                 dma((2,)),
+                dma,
                 dma((n_ep,)),
-                dma((n_ep,)),
-                dma((n_ep,)),
-                dma((n_ep,)),
+                dma,
+                dma((n_ep // 2,)),
+                dma,
                 dma((groups,)),
+                dma,
                 dma((groups,)),
-                dma((groups, 2)),
-                dma((groups, 2)),
-                dma((groups, 2)),
-                dma((groups, 2)),
+                dma,
                 dma((groups,)),
+                dma,
                 dma((groups,)),
-                dma((n_ep,)),
+                dma,
                 dma((n_ep,)),
             ],
             compiler_params=pltpu.CompilerParams(
@@ -654,6 +666,17 @@
             ),
             name="mixer_and_experts",
         )(*inputs)
+    )
+    return tuple(
+        pl.pallas_call(
+            publish,
+            out_shape=results,
+            in_specs=[vmem] * 2,
+            out_specs=(hbm, hbm),
+            scratch_shapes=[dma((2,))],
+            compiler_params=pltpu.CompilerParams(vmem_limit_bytes=1024 * 1024),
+            name="publish",
+        )(mixed, expert_out)
     )
 
 

time: 63.8 us -> 61.4 us (0.962)
  local copies, waits for them, and re-layouts: 1.67 us -> 0 us
    unnamed x2 -> x0, local copies, waits for them, and re-layouts: 1.67 us -> none
    pallas_call x1, Pallas kernels: 60.8 us -> 59.5 us  [local(): pl.pallas_call(functools.partial(kernel, n_ep, n_tp, capacity), out_shape...]
    pallas_call x0 -> x1, Pallas kernels: none -> 1.07 us  [local(): pl.pallas_call(publish, out_shape=results, in_specs=[vmem] * 2, out_specs...]
where the time goes in v2:
time: 61.4 us; the launch traced here: 61.3 us
  Pallas kernels  60.6 us (99%)
  between operations  0.64 us (1%)
    pallas_call x1, Pallas kernels, local(): pl.pallas_call(functools.partial(kernel, n_ep, n_tp, capacity), out_shape...  59.5 us

profile of v2, /device:TPU:0, one launch (start us, length us, event | category | flops | bytes accessed | tf_op | source)
XLA Modules:
  0.0 61.3 jit_solution(7132427377884137874)
XLA Ops:
  0.6 59.5 %mixer_and_experts.1 = (bf16[256,2048]{1,0:T(8,128)(2,1)S(1)}, bf16[256,512]{1,0:T(8,128)(2,1)S(1)}) custom-call(bf16[256,1024]{1,0:T(8,128)(2,1)} %value_hbm.1, bf16[256,1024]{1,0:T(8,128)(2,1)} %gate_hbm.1, f32[31,1024]{1,0:T(8,128)} %taps_hbm.1, f32[1,1024]{1,0:T(1,128)} %bitcast.9, f32[1,1024]{1,0:T(1,128)} %bitcast.10, f32[1,1024]{1,0:T(1,128)} %bitcast.11, ...), custom_call_target="tpu_custom_call" | custom-call | tf_op jit(solution)/shard_map/mixer_and_experts/pallas_call | solution.py:619
  60.2 1.1 %publish.1 = (bf16[256,2048]{1,0:T(8,128)(2,1)}, bf16[256,512]{1,0:T(8,128)(2,1)}) custom-call(bf16[256,2048]{1,0:T(8,128)(2,1)S(1)} %get-tuple-element.4.mixer, bf16[256,512]{1,0:T(8,128)(2,1)S(1)} %get-tuple-element.5.expert), custom_call_target="tpu_custom_call" | custom-call | tf_op jit(solution)/shard_map/publish/pallas_call | solution.py:671

commit v3 on v2

--- a/solution.py
+++ b/solution.py
@@ -12,18 +12,20 @@
 swish_alpha = 1.702
 LANES = 128
 SCHEDULE = (
-    "C0 F0 D0 S1",
+    "H G1 W1 G4",
+    "G2 O R C0",
+    "F0 D0 G5 W2",
     "F1 F2 A1 F3",
-    "A2 S2 C1 F4",
-    "D1 S3 E0 B2",
-    "F5 A4 C2 A3",
-    "F6 D2 B4 C3",
-    "A6 C4 E2 E1",
-    "D4 F7 B6 A5",
-    "C5 A7 C6 E4",
+    "A2 G6 G3 G7",
+    "C1 F4 D1 W3",
+    "E0 B2 F5 A4",
+    "C2 A3 F6 D2",
+    "B4 A6 C3+4 E2",
+    "E1 A5 D4 F7",
+    "B6 A7 C5+6 E4",
     "D6 D3 B7 C7",
-    "E6 D7 D5 E3",
-    "E7 E5",
+    "E6 D5 D7 E3",
+    "E5 E7",
 )
 f32 = jnp.float32
 bf16 = jnp.bfloat16
@@ -31,6 +33,15 @@
 
 def dot(a, b):
     return jnp.dot(a, b, preferred_element_type=f32)
+
+
+def plain_schedule(n_ep, groups):
+    words = ["H"] + [f"G{k}" for k in range(1, n_ep)] + "O R F0 F1 F2 F3 F4 F5 F6 F7".split()
+    for t in range(groups + 4):
+        for stage, lag in (("D", 3), ("E", 4), ("B", 1), ("C", 2), ("A", 0)):
+            if 0 <= t - lag < groups:
+                words.append(f"{stage}{t - lag}")
+    return words
 
 
 def kernel(
@@ -306,31 +317,28 @@
     with jax.named_scope("w_barrier"):
         pl.semaphore_wait(barrier, n_ep + 2 - jnp.where(here == last, 1, 0))
 
-    @pl.when(here < last)
-    def _():
-        halo.start()
-
     @pl.when(here == 0)
     def _():
         halo_in[...] = jnp.zeros_like(halo_in)
 
-    if single and n_ep == 8:
-        staged = ((1, -1, 4, 2), (5, -2), (6, 3), (7, -3))
-    else:
-        staged = (range(1, n_ep),)
-
-    def send(n):
-        for k in staged[n] if n < len(staged) else ():
-            (dispatch(k) if k > 0 else dispatch_wide(-k)).start()
-
-    with jax.named_scope("wide"):
-        send(0)
-    with jax.named_scope("own"):
-        if single:
-            for n in range(n_tp):
-                arrived[n, 0:capacity] = dot(chosen[0:capacity], columns(n)).astype(bf16)
-        else:
-            arrived[q, 0:capacity] = outgoing[0:capacity]
+    def start_halo():
+        @pl.when(here < last)
+        def _():
+            halo.start()
+
+    def send(k):
+        dispatch(k).start()
+
+    def send_wide(k):
+        dispatch_wide(k).start()
+
+    def own():
+        with jax.named_scope("own"):
+            if single:
+                for n in range(n_tp):
+                    arrived[n, 0:capacity] = dot(chosen[0:capacity], columns(n)).astype(bf16)
+            else:
+                arrived[q, 0:capacity] = outgoing[0:capacity]
 
     def gate_tile(l, c):
         at = pl.ds(pl.multiple_of(l * LANES, LANES), LANES)
@@ -505,11 +513,17 @@
         with jax.named_scope(f"F{n}"):
             fillers[n]()
 
-    for name in ("gate_w", "up_w", "down_w"):
-        loads[name].wait()
-    stages = {"A": take, "B": relay, "S": send, "C": compute, "D": halve, "E": finish, "F": fill}
-    for word in " ".join(SCHEDULE).split():
-        stages[word[0]](*[int(n) for n in word[1:].split("+")])
+    def ready():
+        for name in ("gate_w", "up_w", "down_w"):
+            loads[name].wait()
+
+    once = {"H": start_halo, "O": own, "R": ready}
+    stages = {"A": take, "B": relay, "G": send, "W": send_wide, "C": compute, "D": halve, "E": finish, "F": fill}
+    for word in " ".join(SCHEDULE).split() if single and n_ep == 8 else plain_schedule(n_ep, groups):
+        if word in once:
+            once[word]()
+        else:
+            stages[word[0]](*[int(n) for n in word[1:].split("+")])
     returned[0:capacity] = summed[0:capacity]
 
     def came_back(k, c):

time: 61.4 us -> 60.3 us (0.982)
  Pallas kernels: 60.6 us -> 59.5 us
    pallas_call x1, Pallas kernels: 59.5 us -> 58.4 us  [local(): pl.pallas_call(functools.partial(kernel, n_ep, n_tp, capacity), out_shape...]
where the time goes in v3:
time: 60.3 us; the launch traced here: 60.1 us
  Pallas kernels  59.5 us (99%)
  between operations  0.64 us (1%)
    pallas_call x1, Pallas kernels, local(): pl.pallas_call(functools.partial(kernel, n_ep, n_tp, capacity), out_shape...  58.4 us

profile of v3, /device:TPU:0, one launch (start us, length us, event | category | flops | bytes accessed | tf_op | source)
XLA Modules:
  0.0 60.1 jit_solution(12291428744644922296)
XLA Ops:
  0.6 58.4 %mixer_and_experts.1 = (bf16[256,2048]{1,0:T(8,128)(2,1)S(1)}, bf16[256,512]{1,0:T(8,128)(2,1)S(1)}) custom-call(bf16[256,1024]{1,0:T(8,128)(2,1)} %value_hbm.1, bf16[256,1024]{1,0:T(8,128)(2,1)} %gate_hbm.1, f32[31,1024]{1,0:T(8,128)} %taps_hbm.1, f32[1,1024]{1,0:T(1,128)} %bitcast.9, f32[1,1024]{1,0:T(1,128)} %bitcast.10, f32[1,1024]{1,0:T(1,128)} %bitcast.11, ...), custom_call_target="tpu_custom_call" | custom-call | tf_op jit(solution)/shard_map/mixer_and_experts/pallas_call | solution.py:633
  59.1 1.1 %publish.1 = (bf16[256,2048]{1,0:T(8,128)(2,1)}, bf16[256,512]{1,0:T(8,128)(2,1)}) custom-call(bf16[256,2048]{1,0:T(8,128)(2,1)S(1)} %get-tuple-element.4.mixer, bf16[256,512]{1,0:T(8,128)(2,1)S(1)} %get-tuple-element.5.expert), custom_call_target="tpu_custom_call" | custom-call | tf_op jit(solution)/shard_map/publish/pallas_call | solution.py:685

commit v4 on v3

--- a/solution.py
+++ b/solution.py
@@ -36,7 +36,7 @@
 
 
 def plain_schedule(n_ep, groups):
-    words = ["H"] + [f"G{k}" for k in range(1, n_ep)] + "O R F0 F1 F2 F3 F4 F5 F6 F7".split()
+    words = ["H"] + [f"G{k}" for k in range(1, n_ep)] + ["O", "R"] + [f"F{n}" for n in range(8)]
     for t in range(groups + 4):
         for stage, lag in (("D", 3), ("E", 4), ("B", 1), ("C", 2), ("A", 0)):
             if 0 <= t - lag < groups:

time: 60.3 us -> 60.3 us (level)
  no operation moved by 1% of the time
where the time goes in v4:
time: 60.3 us; the launch traced here: 60.1 us
  Pallas kernels  59.5 us (99%)
  between operations  0.64 us (1%)
    pallas_call x1, Pallas kernels, local(): pl.pallas_call(functools.partial(kernel, n_ep, n_tp, capacity), out_shape...  58.4 us

profile of v4, /device:TPU:0, one launch (start us, length us, event | category | flops | bytes accessed | tf_op | source)
XLA Modules:
  0.0 60.1 jit_solution(12291428744644922296)
XLA Ops:
  0.6 58.4 %mixer_and_experts.1 = (bf16[256,2048]{1,0:T(8,128)(2,1)S(1)}, bf16[256,512]{1,0:T(8,128)(2,1)S(1)}) custom-call(bf16[256,1024]{1,0:T(8,128)(2,1)} %value_hbm.1, bf16[256,1024]{1,0:T(8,128)(2,1)} %gate_hbm.1, f32[31,1024]{1,0:T(8,128)} %taps_hbm.1, f32[1,1024]{1,0:T(1,128)} %bitcast.9, f32[1,1024]{1,0:T(1,128)} %bitcast.10, f32[1,1024]{1,0:T(1,128)} %bitcast.11, ...), custom_call_target="tpu_custom_call" | custom-call | tf_op jit(solution)/shard_map/mixer_and_experts/pallas_call | solution.py:633
  59.1 1.1 %publish.1 = (bf16[256,2048]{1,0:T(8,128)(2,1)}, bf16[256,512]{1,0:T(8,128)(2,1)}) custom-call(bf16[256,2048]{1,0:T(8,128)(2,1)S(1)} %get-tuple-element.4.mixer, bf16[256,512]{1,0:T(8,128)(2,1)S(1)} %get-tuple-element.5.expert), custom_call_target="tpu_custom_call" | custom-call | tf_op jit(solution)/shard_map/publish/pallas_call | solution.py:685
